TPU v7x, 32 devices: a whole 2x2x4 slice. The times are simulated.
32 devices in a mesh: ep: 4 (over y, x), tp: 8 (over z, core).
Axes of the slice: x: 2, y: 2, z: 4, core: 2. Of those that a mesh axis runs over, the one named last changes fastest.
Arguments:
- query_heads: bfloat16 [1024, 2048], P('ep', 'tp'), may hold values from -60 to 60
- key_heads: bfloat16 [1024, 2048], P('ep', 'tp'), may hold values from -40.5 to 40.5
- value_heads: bfloat16 [1024, 2048], P('ep', 'tp'), may hold values from -6 to 6
- diff_lambda: float32 [16], P('tp'), may hold values from 0.3 to 0.8
- sub_gain: float32 [128], replicated, may hold values from 0.1 to 1.9
- out_weight: bfloat16 [2048, 4096], P('tp'), may hold values from -0.125 to 0.125
- routed_input: bfloat16 [1024, 4096], P('ep', 'tp'), may hold values from -40 to 40
- routes: int32 [1024, 2], P('ep'), may hold values from 0 to 3, all different within a row; in each aligned block of 256 rows (0 to 255, 256 to 511, ...) at most 256 rows name the same one
- route_weights: float32 [1024, 2], P('ep'), may hold values from 0.3 to 1.5
- expert_gate: bfloat16 [4, 4096, 4096], P('ep', None, 'tp'), may hold values from -0.09375 to 0.09375
- expert_up: bfloat16 [4, 4096, 4096], P('ep', None, 'tp'), may hold values from -0.09375 to 0.09375
- expert_down: bfloat16 [4, 4096, 4096], P('ep', 'tp'), may hold values from -0.09375 to 0.09375
- shared_gate: bfloat16 [4096, 2048], P(None, 'tp'), may hold values from -0.09375 to 0.09375
- shared_up: bfloat16 [4096, 2048], P(None, 'tp'), may hold values from -0.09375 to 0.09375
- shared_down: bfloat16 [2048, 4096], P('tp'), may hold values from -0.125 to 0.125
Outputs:
- mixer_output: bfloat16 [1024, 4096], P('ep', 'tp')
- routed_output: bfloat16 [1024, 4096], P('ep', 'tp')
Inputs may be any that keep to these rules, and one draw needn't show every extreme that they name: `routes`: each row names 2 different experts. In each aligned block of 256 rows no expert is named by more than 256 rows, a bound that some block reaches.
All inputs are finite; a program needn't handle non-finite values.
Results may differ from a plain program's by a relative error of at most 0.02.
Values may be sent and summed in bfloat16 or wider, within the bound.
A program may use at most 128 MiB of HBM per device.

v0:
```python
import jax
import jax.numpy as jnp
from jax import lax
from jax.sharding import PartitionSpec as P

ROPE_BASE = 10000.0
NORM_EPS = 1e-06
MASKED = -1e30


def rotate(values, positions):
    half_width = values.shape[-1] // 2
    inverse_freq = ROPE_BASE ** (-jnp.arange(half_width, dtype=jnp.float32) / half_width)
    angles = positions.astype(jnp.float32)[:, None] * inverse_freq[None, :]
    angles = angles.reshape((angles.shape[0],) + (1,) * (values.ndim - 2) + (half_width,))
    cosine = jnp.cos(angles)
    sine_part = jnp.sin(angles)
    lower = values[..., :half_width]
    upper = values[..., half_width:]
    return jnp.concatenate(
        [lower * cosine - upper * sine_part, upper * cosine + lower * sine_part], axis=-1
    )


def mixer_terms(query_heads, key_heads, value_heads, diff_lambda, sub_gain, out_weight):
    row_count = query_heads.shape[0]
    local_heads = diff_lambda.shape[0]
    value_width = value_heads.shape[1] // local_heads
    key_width = query_heads.shape[1] // (2 * local_heads)
    score_scale = key_width ** (-0.5)
    offset = lax.axis_index("ep") * row_count
    positions = offset + jnp.arange(row_count, dtype=jnp.int32)
    last_row = offset + row_count - 1
    query_rot = rotate(
        query_heads.astype(jnp.float32).reshape(row_count, local_heads, 2, key_width), positions
    ).astype(jnp.bfloat16)
    queries = jnp.transpose(query_rot, (1, 2, 0, 3))
    key_rot = (
        rotate(
            key_heads.astype(jnp.float32).reshape(row_count, local_heads, 2, key_width), positions
        )
        .astype(jnp.bfloat16)
        .reshape(row_count, local_heads * 2 * key_width)
    )
    start_state = (
        jnp.full((local_heads, 2, row_count), MASKED, jnp.float32),
        jnp.zeros((local_heads, 2, row_count), jnp.float32),
        jnp.zeros((local_heads, 2, row_count, value_width), jnp.float32),
    )
    carried = start_state
    key_piece = lax.all_gather(key_rot, "ep", axis=0, tiled=True)
    value_piece = lax.all_gather(value_heads, "ep", axis=0, tiled=True)
    piece_rows = key_piece.shape[0]
    key_block = 512
    block_count = piece_rows // key_block
    key_blocks = key_piece.reshape(block_count, key_block, local_heads, 2, key_width)
    value_blocks = value_piece.reshape(block_count, key_block, local_heads, value_width)

    def block_step(running, block_item):
        key_rows, value_rows, block_index = block_item
        block_start = block_index * key_block

        def attend_block(partial_state):
            maxima, totals, weighted = partial_state
            key_positions = block_start + jnp.arange(key_block, dtype=jnp.int32)
            visible = key_positions[None, :] <= positions[:, None]
            scores = (
                jnp.einsum("hmqd,khmd->hmqk", queries, key_rows, preferred_element_type=jnp.float32)
                * score_scale
            )
            scores = jnp.where(visible, scores, MASKED)
            new_maxima = jnp.maximum(maxima, jnp.max(scores, axis=3))
            exp_weights = jnp.where(visible, jnp.exp(scores - new_maxima[..., None]), 0.0)
            shrink = jnp.exp(maxima - new_maxima)
            new_totals = totals * shrink + jnp.sum(exp_weights, axis=3)
            update = jnp.einsum(
                "hmqk,khw->hmqw",
                exp_weights.astype(jnp.bfloat16),
                value_rows,
                preferred_element_type=jnp.float32,
            )
            return (new_maxima, new_totals, weighted * shrink[..., None] + update)

        return (
            lax.cond(
                block_start <= last_row, attend_block, lambda partial_state: partial_state, running
            ),
            None,
        )

    carried, _ = lax.scan(
        block_step, carried, (key_blocks, value_blocks, jnp.arange(block_count, dtype=jnp.int32))
    )
    maxima, totals, weighted = carried
    attended = weighted / totals[..., None]
    mixed_heads = attended[:, 0] - diff_lambda[:, None, None] * attended[:, 1]
    normed = (
        mixed_heads
        * lax.rsqrt(jnp.mean(mixed_heads * mixed_heads, axis=2, keepdims=True) + NORM_EPS)
        * sub_gain
    )
    heads_out = jnp.transpose(normed.astype(jnp.bfloat16), (1, 0, 2)).reshape(
        row_count, local_heads * value_width
    )
    return jnp.dot(heads_out, out_weight, preferred_element_type=jnp.float32)


def expert_terms(
    routed_input, routes, expert_gate, expert_up, expert_down, shared_gate, shared_up, shared_down
):
    row_count, part_width = routed_input.shape
    top_count = routes.shape[1]
    local_experts = expert_gate.shape[0]
    groups = lax.axis_size("ep")
    experts = local_experts * groups
    capacity = 2 * row_count * top_count // experts
    copies = row_count * top_count
    flat_routes = routes.reshape(copies)
    onehot = (flat_routes[:, None] == jnp.arange(experts, dtype=jnp.int32)[None, :]).astype(
        jnp.int32
    )
    rank_within = jnp.sum((jnp.cumsum(onehot, axis=0) - onehot) * onehot, axis=1)
    slot_index = flat_routes * capacity + rank_within
    placer = (
        slot_index[:, None] == jnp.arange(experts * capacity, dtype=jnp.int32)[None, :]
    ).astype(jnp.bfloat16)
    token_slots = jnp.sum(placer.reshape(row_count, top_count, experts * capacity), axis=1)
    outgoing = jnp.dot(token_slots.T, routed_input, preferred_element_type=jnp.float32).astype(
        jnp.bfloat16
    )
    arrived = lax.all_to_all(
        outgoing.reshape(groups, local_experts * capacity, part_width),
        "ep",
        split_axis=0,
        concat_axis=0,
        tiled=True,
    )
    slot_count = groups * capacity
    slot_rows = jnp.transpose(
        arrived.reshape(groups, local_experts, capacity, part_width), (1, 0, 2, 3)
    ).reshape(local_experts, slot_count, part_width)
    slot_piece = lax.all_gather(slot_rows, "tp", axis=2, tiled=True)
    own_piece = lax.all_gather(routed_input[None], "tp", axis=2, tiled=True)
    own_rows = own_piece[0]
    gate_sum = jnp.einsum(
        "emc,ecf->emf", slot_piece, expert_gate, preferred_element_type=jnp.float32
    )
    up_sum = jnp.einsum("emc,ecf->emf", slot_piece, expert_up, preferred_element_type=jnp.float32)
    square_sum = jnp.sum(jnp.square(slot_piece.astype(jnp.float32)), axis=2)
    shared_gate_sum = jnp.dot(own_rows, shared_gate, preferred_element_type=jnp.float32)
    shared_up_sum = jnp.dot(own_rows, shared_up, preferred_element_type=jnp.float32)
    shared_square = jnp.sum(jnp.square(own_rows.astype(jnp.float32)), axis=1)
    full_width = expert_gate.shape[1]
    factor = lax.rsqrt(square_sum / full_width + NORM_EPS)[..., None]
    hidden = (jax.nn.silu(gate_sum * factor) * (up_sum * factor)).astype(jnp.bfloat16)
    shared_factor = lax.rsqrt(shared_square / full_width + NORM_EPS)[:, None]
    shared_hidden = (
        jax.nn.silu(shared_gate_sum * shared_factor) * (shared_up_sum * shared_factor)
    ).astype(jnp.bfloat16)
    shared_terms = jnp.dot(shared_hidden, shared_down, preferred_element_type=jnp.float32)
    routed_terms = jnp.einsum(
        "emf,efd->emd", hidden, expert_down, preferred_element_type=jnp.float32
    )
    routed_sum = lax.psum_scatter(
        routed_terms.astype(jnp.bfloat16), "tp", scatter_dimension=2, tiled=True
    ).astype(jnp.float32)
    return (routed_sum, shared_terms, placer)


def expert_finish(routed_sum, shared_sum, placer, route_weights):
    local_experts, slot_count, part_width = routed_sum.shape
    groups = lax.axis_size("ep")
    capacity = slot_count // groups
    leaving = jnp.transpose(
        routed_sum.astype(jnp.bfloat16).reshape(local_experts, groups, capacity, part_width),
        (1, 0, 2, 3),
    ).reshape(groups, local_experts * capacity, part_width)
    returned = lax.all_to_all(leaving, "ep", split_axis=0, concat_axis=0, tiled=True)
    copy_results = jnp.dot(
        placer,
        returned.reshape(groups * local_experts * capacity, part_width),
        preferred_element_type=jnp.float32,
    )
    row_count, top_count = route_weights.shape
    routed = jnp.sum(
        copy_results.reshape(row_count, top_count, part_width) * route_weights[:, :, None], axis=1
    )
    return (routed + shared_sum).astype(jnp.bfloat16)


def body(
    query_heads,
    key_heads,
    value_heads,
    diff_lambda,
    sub_gain,
    out_weight,
    routed_input,
    routes,
    route_weights,
    expert_gate,
    expert_up,
    expert_down,
    shared_gate,
    shared_up,
    shared_down,
):
    mixer_partial = mixer_terms(
        query_heads, key_heads, value_heads, diff_lambda, sub_gain, out_weight
    )
    routed_sum, shared_terms, placer = expert_terms(
        routed_input,
        routes,
        expert_gate,
        expert_up,
        expert_down,
        shared_gate,
        shared_up,
        shared_down,
    )
    mixer_sum, shared_sum = (
        lax.psum_scatter(
            mixer_partial.astype(jnp.bfloat16), "tp", scatter_dimension=1, tiled=True
        ).astype(jnp.float32),
        lax.psum_scatter(
            shared_terms.astype(jnp.bfloat16), "tp", scatter_dimension=1, tiled=True
        ).astype(jnp.float32),
    )
    return (
        mixer_sum.astype(jnp.bfloat16),
        expert_finish(routed_sum, shared_sum, placer, route_weights),
    )


def solution(mesh):
    placed = (
        P("ep", "tp"),
        P("ep", "tp"),
        P("ep", "tp"),
        P("tp"),
        P(),
        P("tp", None),
        P("ep", "tp"),
        P("ep", None),
        P("ep", None),
        P("ep", None, "tp"),
        P("ep", None, "tp"),
        P("ep", "tp", None),
        P(None, "tp"),
        P(None, "tp"),
        P("tp", None),
    )
    return jax.shard_map(
        body, mesh=mesh, in_specs=placed, out_specs=(P("ep", "tp"), P("ep", "tp")), check_vma=False
    )
```

profile of v0, /device:TPU:0, one launch (start us, length us, event | category | flops | bytes accessed | tf_op | source)
XLA Modules:
  0.0 315.3 jit_solution(10947524529678196263)
XLA Ops:
  7.2 0.9 copy.54
  8.5 1.2 reduce-window.6
  10.4 0.7 multiply_add_fusion.1
  11.4 1.4 convolution_convert_fusion.2
  12.8 19.2 %all_to_all.10 = bf16[4,256,512]{2,1,0:T(8,128)(2,1)} all-to-all(bf16[4,256,512]{2,1,0:T(8,128)(2,1)S(1)} %bitcast.120), channel_id=1, replica_groups=mesh['ep'=4,'tp'=8] {'ep'}, dimensions={0} | all-to-all | bytes 2097152 | tf_op jit(solution)/shard_map/all_to_all | solution.py:131
  32.1 0.7 all-gather.6.cloned.1.call-update
  32.9 81.1 %all-gather.4.cloned.1.call-done = bf16[1,1024,4096]{2,1,0:T(8,128)(2,1)} async-done(((bf16[1,1024,512]{2,1,0:T(8,128)(2,1)}), bf16[1,1024,4096]{2,1,0:T(8,128)(2,1)}) %all-gather.4.cloned.1.call-update) | async-done | bytes 8388624 | tf_op jit(solution)/shard_map/all_gather | solution.py:142
  114.0 5.2 %multiply_reduce_fusion = f32[1024]{0:T(1024)S(1)} fusion(bf16[1,1024,4096]{2,1,0:T(8,128)(2,1)} %all-gather.4.cloned.1.call-done), kind=kLoop, calls=%fused_computation.26 | loop fusion | flops 12581888 | bytes 8392704 | tf_op jit(solution)/shard_map/reduce_sum | solution.py:149
  119.8 8.1 %fusion.20 = f32[1024,512]{1,0:T(8,128)} fusion(bf16[1,1024,4096]{2,1,0:T(8,128)(2,1)S(1)} %copy-done.2, bf16[1,4096,512]{2,1,0:T(8,128)(2,1)} %param.29), kind=kOutput, calls=%fused_computation.27 | convolution fusion | flops 4294967296 | bytes 14680064 | tf_op jit(solution)/shard_map/emc,ecf->emf/dot_general | solution.py:148
  127.9 16.5 %convert_bitcast_fusion = bf16[1,1024,4096]{2,1,0:T(8,128)(2,1)} fusion(bf16[1,512,4096]{2,1,0:T(8,128)(2,1)} %param.30, f32[1024,512]{1,0:T(8,128)} %fusion.20, bf16[1,4096,512]{2,1,0:T(8,128)(2,1)} %param.28, bf16[1,1024,4096]{2,1,0:T(8,128)(2,1)} %all-gather.4.cloned.1.call-done, f32[1024]{0:T(1024)S(1)} %add_rsqrt_fusion), kind=kOutput, calls=%fused_computation.31 | convolution fusion | flops 8598323200 | bytes 27267072 | tf_op jit(solution)/shard_map/emf,efd->emd/dot_general | solution.py:161
  144.6 2.2 multiply_reduce_fusion.1
  146.9 2.3 convolution_multiply_fusion.1
  149.2 6.5 %convolution_convert_fusion = bf16[256,4096]{1,0:T(8,128)(2,1)} fusion(bf16[256,4096]{1,0:T(8,128)(2,1)S(1)} %copy-done, bf16[256,4096]{1,0:T(8,128)(2,1)} %all-gather.6.cloned.1.call-done, bf16[4096,256]{1,0:T(8,128)(2,1)} %param.32, f32[256,256]{1,0:T(8,128)S(1)} %convolution_multiply_fusion.1, f32[256]{0:T(256)S(1)} %add_rsqrt_fusion.2), kind=kOutput, calls=%fused_computation.32 | convolution fusion | flops 1075249152 | bytes 8651776 | tf_op jit(solution)/shard_map/dot_general | solution.py:160
  155.8 0.8 copy-done.5
  157.2 14.2 %all_gather.12 = bf16[1024,256]{0,1:T(8,128)(2,1)S(1)} all-gather(bf16[256,256]{0,1:T(8,128)(2,1)S(1)} %bitcast.127), channel_id=1, replica_groups=mesh['ep'=4,'tp'=8] {'ep'}, dimensions={0}, use_global_device_ids=true | all-gather | bytes 655360 | tf_op jit(solution)/shard_map/all_gather | solution.py:51
  171.8 10.2 %all_gather.13 = bf16[1024,256]{1,0:T(8,128)(2,1)S(1)} all-gather(bf16[256,256]{1,0:T(8,128)(2,1)S(1)} %copy-done.7), channel_id=1, replica_groups=mesh['ep'=4,'tp'=8] {'ep'}, dimensions={0}, use_global_device_ids=true | all-gather | bytes 655360 | tf_op jit(solution)/shard_map/all_gather | solution.py:52
  182.1 0.9 reshape.227
  183.0 1.9 copy.51
  185.0 4.9 %while.15 = (s32[]{:T(128)}, f32[2,2,256]{2,1,0:T(2,128)S(1)}, f32[2,2,256]{2,1,0:T(2,128)S(1)}, f32[2,2,256,128]{3,2,1,0:T(8,128)S(1)}, s32[2]{0:T(128)S(1)}, /...) while((s32[]{:T(128)}, f32[2,2,256]{2,1,0:T(2,128)S(1)}, ...), condition=%wide.region_5.6_spmd.clone, body=%wide.region_0.5_spmd.clone.sunk | while | flops 208538368 | bytes 10690895 | solution.py:91
  185.1 0.6 dynamic_slice.34
  186.3 2.3 conditional.3
  186.5 0.6 fusion.2
  187.6 1.0 convolution_add_fusion
  188.6 0.6 dynamic_slice.34
  190.8 0.9 copy-done.3
  191.7 2.0 convolution_convert_fusion.1
  193.8 40.7 %reduce-scatter.6.cloned.1.call-done = bf16[1,1024,512]{2,1,0:T(8,128)(2,1)} async-done(((bf16[1,1024,4096]{2,1,0:T(8,128)(2,1)}), bf16[1,1024,512]{2,1,0:T(8,128)(2,1)}) %reduce-scatter.6.cloned.1.call-update) | async-done | bytes 1048592 | tf_op jit(solution)/shard_map/reduce_scatter | solution.py:164
  234.5 16.0 %all_to_all.11 = bf16[4,256,512]{2,1,0:T(8,128)(2,1)S(1)} all-to-all(bf16[4,256,512]{2,1,0:T(8,128)(2,1)} %bitcast.122), channel_id=1, replica_groups=mesh['ep'=4,'tp'=8] {'ep'}, dimensions={0} | all-to-all | bytes 2097152 | tf_op jit(solution)/shard_map/all_to_all | solution.py:178
  250.5 0.8 fusion.42
  251.3 20.0 %reduce-scatter.8.cloned.1.call-done = bf16[256,512]{1,0:T(8,128)(2,1)} async-done(((bf16[256,4096]{1,0:T(8,128)(2,1)}), bf16[256,512]{1,0:T(8,128)(2,1)}) %reduce-scatter.8.cloned.1.call-update) | async-done | bytes 262160 | tf_op jit(solution)/shard_map/reduce_scatter | solution.py:225
  271.3 1.7 add_convert_fusion
  273.0 35.7 %reduce-scatter.4.cloned.1.call-done = bf16[256,512]{1,0:T(8,128)(2,1)} async-done(((bf16[256,4096]{1,0:T(8,128)(2,1)}), bf16[256,512]{1,0:T(8,128)(2,1)}) %reduce-scatter.4.cloned.1.call-update) | async-done | bytes 262160 | tf_op jit(solution)/shard_map/reduce_scatter | solution.py:222
  (72 shorter events, 4.9 us)
Async XLA Ops:
  7.2 142.0 %copy-start = (bf16[256,4096]{1,0:T(8,128)(2,1)S(1)}, bf16[256,4096]{1,0:T(8,128)(2,1)}, u32[]{:S(2)}) copy-start(bf16[256,4096]{1,0:T(8,128)(2,1)} %param.33) | copy-start | bytes 6291460
  7.2 106.8 %all-gather.4.cloned.1.call-start = ((), (), s32[]{:S(2)}) async-start(), calls=%async_computation.6 | async-start | bytes 9437184 | tf_op jit(solution)/shard_map/all_gather | solution.py:142
  32.1 112.5 %all-gather.6.cloned.1.call-start = ((), (), s32[]{:S(2)}) async-start(), calls=%async_computation.9 | async-start | bytes 2359296 | tf_op jit(solution)/shard_map/all_gather | solution.py:143
  32.8 201.7 %reduce-scatter.6.cloned.1.call-start = ((), (), s32[]{:S(2)}) async-start(), calls=%async_computation.7 | async-start | bytes 9437184 | tf_op jit(solution)/shard_map/reduce_scatter | solution.py:164
  114.0 5.8 %copy-start.2 = (bf16[1,1024,4096]{2,1,0:T(8,128)(2,1)S(1)}, bf16[1,1024,4096]{2,1,0:T(8,128)(2,1)}, u32[]{:S(2)}) copy-start(bf16[1,1024,4096]{2,1,0:T(8,128)(2,1)} %all-gather.4.cloned.1.call-done) | copy-start | bytes 25165828
  144.4 127.0 %reduce-scatter.8.cloned.1.call-start = ((), (), s32[]{:S(2)}) async-start(), calls=%async_computation.8 | async-start | bytes 2359296 | tf_op jit(solution)/shard_map/reduce_scatter | solution.py:225
  144.6 2.3 copy-start.1
  155.7 0.9 copy-start.5
  155.7 1.0 copy-start.6
  155.8 153.0 %reduce-scatter.4.cloned.1.call-start = ((), (), s32[]{:S(2)}) async-start(), calls=%async_computation.5 | async-start | bytes 2359296 | tf_op jit(solution)/shard_map/reduce_scatter | solution.py:222
  156.8 15.1 %copy-start.7 = (bf16[256,256]{1,0:T(8,128)(2,1)S(1)}, bf16[256,256]{1,0:T(8,128)(2,1)}, u32[]{:S(2)}) copy-start(bf16[256,256]{1,0:T(8,128)(2,1)} %param.21) | copy-start | bytes 393220
  186.5 1.1 copy-start.4
  189.9 0.7 copy-start.8
  189.9 0.8 copy-start.9
  190.1 1.6 copy-start.3
  193.8 56.8 %copy-start.10 = (f32[256,2]{0,1:T(2,128)S(1)}, f32[256,2]{0,1:T(2,128)}, u32[]{:S(2)}) copy-start(f32[256,2]{0,1:T(2,128)} %param.27) | copy-start | bytes 6148
Sparse Core Ops, SparseCore 0:
  32.2 81.7 all-gather.3
  115.6 27.6 all-gather.5
  145.6 88.8 reduce-scatter.5
  236.7 34.6 reduce-scatter.7
  274.0 34.6 reduce-scatter.3
where the time goes:
time: 316 us; the launch traced here: 315 us
  waiting for transfers between devices  178 us (56%)
  blocking collectives  59.7 us (19%)
  matrix products  39.2 us (12%)
  between operations  14.1 us (4%)
  other arithmetic  12.9 us (4%)
  local copies, waits for them, and re-layouts  9.29 us (3%)
    all_gather x1, waiting for transfers between devices, expert_terms(): slot_piece = lax.all_gather(slot_rows, 'tp', axis=2, tiled=True)  81.1 us
    reduce_scatter x1, waiting for transfers between devices, expert_terms(): lax.psum_scatter(routed_terms.astype(jnp.bfloat16), 'tp', scatter_dimensi...  40.7 us
    reduce_scatter x1, waiting for transfers between devices, body(): lax.psum_scatter(mixer_partial.astype(jnp.bfloat16), 'tp', scatter_dimens...  35.7 us
    reduce_scatter x1, waiting for transfers between devices, body(): lax.psum_scatter(shared_terms.astype(jnp.bfloat16), 'tp', scatter_dimensi...  20 us
    all_to_all x1, blocking collectives, expert_terms(): lax.all_to_all(outgoing.reshape(groups, local_experts * capacity, part_wi...  19.2 us
    dot_general x1, matrix products, expert_terms(): jnp.einsum('emf,efd->emd', hidden, expert_down, preferred_element_type=jn...  16.5 us
    all_to_all x1, blocking collectives, expert_finish(): lax.all_to_all(leaving, 'ep', split_axis=0, concat_axis=0, tiled=True)  16 us
    all_gather x1, blocking collectives, mixer_terms(): key_piece = lax.all_gather(key_rot, 'ep', axis=0, tiled=True)  14.2 us
  transfers between devices with their start and end apart: 5, of which 4 were waited for; matrix products, arithmetic and copies ran while one was open for 17% of the time, Pallas kernels for 0%

commit v1 on v0

--- a/solution.py
+++ b/solution.py
@@ -2,6 +2,7 @@
 import jax.numpy as jnp
 from jax import lax
 from jax.sharding import PartitionSpec as P
+from jax.lax import all_gather
 
 ROPE_BASE = 10000.0
 NORM_EPS = 1e-06
@@ -23,6 +24,16 @@
 
 
 def mixer_terms(query_heads, key_heads, value_heads, diff_lambda, sub_gain, out_weight):
+
+    def wrap_task(patch, sample):
+        return jnp.split(
+            all_gather(
+                jnp.concatenate([patch, sample], axis=1), axis_name="ep", axis=0, tiled=True
+            ),
+            [patch.shape[1]],
+            axis=1,
+        )
+
     row_count = query_heads.shape[0]
     local_heads = diff_lambda.shape[0]
     value_width = value_heads.shape[1] // local_heads
@@ -48,8 +59,7 @@
         jnp.zeros((local_heads, 2, row_count, value_width), jnp.float32),
     )
     carried = start_state
-    key_piece = lax.all_gather(key_rot, "ep", axis=0, tiled=True)
-    value_piece = lax.all_gather(value_heads, "ep", axis=0, tiled=True)
+    key_piece, value_piece = wrap_task(key_rot, value_heads)
     piece_rows = key_piece.shape[0]
     key_block = 512
     block_count = piece_rows // key_block

time: 316 us -> 345 us (1.092)
  waiting for transfers between devices: 178 us -> 227 us
  blocking collectives: 59.7 us -> 35.4 us
  local copies, waits for them, and re-layouts: 9.29 us -> 13.1 us
    reduce_scatter x1, waiting for transfers between devices: 40.7 us -> 75 us  [expert_terms(): lax.psum_scatter(routed_terms.astype(jnp.bfloat16), 'tp', scatter_dimensi...]
    all_gather x2 -> x0, blocking collectives: 24.4 us -> none  [the longest x1 14.2 us: mixer_terms(): key_piece = lax.all_gather(key_rot, 'ep', axis=0, tiled=True)]
    all_gather x0 -> x1, waiting for transfers between devices: none -> 16.3 us  [wrap_task(): all_gather(jnp.concatenate([patch, sample], axis=1), axis_name='ep', axis...]
  transfers between devices with their start and end apart: 5 -> 6, of which waited for: 4 -> 5; matrix products, arithmetic and copies ran while one was open for 17% -> 17% of each run, Pallas kernels for 0% -> 0%
where the time goes in v1:
time: 345 us; the launch traced here: 344 us
  waiting for transfers between devices  227 us (66%)
  matrix products  38.6 us (11%)
  blocking collectives  35.4 us (10%)
  between operations  14.4 us (4%)
  other arithmetic  13.7 us (4%)
  local copies, waits for them, and re-layouts  13.1 us (4%)
    all_gather x1, waiting for transfers between devices, expert_terms(): slot_piece = lax.all_gather(slot_rows, 'tp', axis=2, tiled=True)  79.6 us
    reduce_scatter x1, waiting for transfers between devices, expert_terms(): lax.psum_scatter(routed_terms.astype(jnp.bfloat16), 'tp', scatter_dimensi...  75 us
    reduce_scatter x1, waiting for transfers between devices, body(): lax.psum_scatter(mixer_partial.astype(jnp.bfloat16), 'tp', scatter_dimens...  35.6 us
    reduce_scatter x1, waiting for transfers between devices, body(): lax.psum_scatter(shared_terms.astype(jnp.bfloat16), 'tp', scatter_dimensi...  19.9 us
    all_to_all x1, blocking collectives, expert_terms(): lax.all_to_all(outgoing.reshape(groups, local_experts * capacity, part_wi...  19.4 us
    dot_general x1, matrix products, expert_terms(): jnp.einsum('emf,efd->emd', hidden, expert_down, preferred_element_type=jn...  16.4 us
    all_gather x1, waiting for transfers between devices, wrap_task(): all_gather(jnp.concatenate([patch, sample], axis=1), axis_name='ep', axis...  16.3 us
    all_to_all x1, blocking collectives, expert_finish(): lax.all_to_all(leaving, 'ep', split_axis=0, concat_axis=0, tiled=True)  16 us
  transfers between devices with their start and end apart: 6, of which 5 were waited for; matrix products, arithmetic and copies ran while one was open for 17% of the time, Pallas kernels for 0%

profile of v1, /device:TPU:0, one launch (start us, length us, event | category | flops | bytes accessed | tf_op | source)
XLA Modules:
  0.0 344.4 jit_solution(6733491308956650615)
XLA Ops:
  7.2 0.9 copy.61
  8.5 1.2 reduce-window.6
  10.4 0.7 multiply_add_fusion.1
  11.4 1.4 convolution_convert_fusion.2
  12.8 19.4 %all_to_all.10 = bf16[4,256,512]{2,1,0:T(8,128)(2,1)} all-to-all(bf16[4,256,512]{2,1,0:T(8,128)(2,1)S(1)} %bitcast.118), channel_id=1, replica_groups=mesh['ep'=4,'tp'=8] {'ep'}, dimensions={0} | all-to-all | bytes 2097152 | tf_op jit(solution)/shard_map/all_to_all | solution.py:141
  32.3 0.7 all-gather.9.cloned.1.call-update
  33.7 0.7 pad_maximum_fusion
  34.5 79.6 %all-gather.7.cloned.1.call-done = bf16[1,1024,4096]{2,1,0:T(8,128)(2,1)} async-done(((bf16[1,1024,512]{2,1,0:T(8,128)(2,1)}), bf16[1,1024,4096]{2,1,0:T(8,128)(2,1)}) %all-gather.7.cloned.1.call-update) | async-done | bytes 8388624 | tf_op jit(solution)/shard_map/all_gather | solution.py:152
  114.2 5.2 %multiply_reduce_fusion = f32[1024]{0:T(1024)S(1)} fusion(bf16[1,1024,4096]{2,1,0:T(8,128)(2,1)} %all-gather.7.cloned.1.call-done), kind=kLoop, calls=%fused_computation.26 | loop fusion | flops 12581888 | bytes 8392704 | tf_op jit(solution)/shard_map/reduce_sum | solution.py:159
  119.9 8.1 %fusion.20 = f32[1024,512]{1,0:T(8,128)} fusion(bf16[1,1024,4096]{2,1,0:T(8,128)(2,1)S(1)} %copy-done.2, bf16[1,4096,512]{2,1,0:T(8,128)(2,1)} %param.29), kind=kOutput, calls=%fused_computation.27 | convolution fusion | flops 4294967296 | bytes 14680064 | tf_op jit(solution)/shard_map/emc,ecf->emf/dot_general | solution.py:158
  128.1 16.4 %convert_bitcast_fusion = bf16[1,1024,4096]{2,1,0:T(8,128)(2,1)} fusion(bf16[1,512,4096]{2,1,0:T(8,128)(2,1)} %param.30, f32[1024,512]{1,0:T(8,128)} %fusion.20, bf16[1,4096,512]{2,1,0:T(8,128)(2,1)} %param.28, bf16[1,1024,4096]{2,1,0:T(8,128)(2,1)} %all-gather.7.cloned.1.call-done, f32[1024]{0:T(1024)S(1)} %add_rsqrt_fusion), kind=kOutput, calls=%fused_computation.31 | convolution fusion | flops 8598323200 | bytes 27267072 | tf_op jit(solution)/shard_map/emf,efd->emd/dot_general | solution.py:171
  144.8 2.2 multiply_reduce_fusion.1
  147.1 2.3 convolution_multiply_fusion.1
  149.4 6.0 %convolution_convert_fusion = bf16[256,4096]{1,0:T(8,128)(2,1)} fusion(bf16[256,4096]{1,0:T(8,128)(2,1)S(1)} %copy-done, bf16[256,4096]{1,0:T(8,128)(2,1)} %all-gather.9.cloned.1.call-done, bf16[4096,256]{1,0:T(8,128)(2,1)} %param.32, f32[256,256]{1,0:T(8,128)S(1)} %convolution_multiply_fusion.1, f32[256]{0:T(256)S(1)} %add_rsqrt_fusion.2), kind=kOutput, calls=%fused_computation.32 | convolution fusion | flops 1075249152 | bytes 8651776 | tf_op jit(solution)/shard_map/dot_general | solution.py:170
  155.5 16.3 %all-gather.5.cloned.1.call-done = bf16[1024,512]{1,0:T(8,128)(2,1)} async-done(((bf16[256,512]{1,0:T(8,128)(2,1)}), bf16[1024,512]{1,0:T(8,128)(2,1)}) %all-gather.5.cloned.1.call-update) | async-done | bytes 1048592 | tf_op jit(solution)/shard_map/all_gather | solution.py:30
  171.8 2.1 fusion.66
  173.9 1.4 reshape.244
  175.3 2.4 copy.57
  177.6 1.2 reshape.227
  178.8 0.9 copy.58
  179.8 4.9 %while.15 = (s32[]{:T(128)}, f32[2,2,256]{2,1,0:T(2,128)S(1)}, f32[2,2,256]{2,1,0:T(2,128)S(1)}, f32[2,2,256,128]{3,2,1,0:T(8,128)S(1)}, s32[2]{0:T(128)S(1)}, /...) while((s32[]{:T(128)}, f32[2,2,256]{2,1,0:T(2,128)S(1)}, ...), condition=%wide.region_5.6_spmd.clone, body=%wide.region_0.5_spmd.clone.sunk | while | flops 208538368 | bytes 10690895 | solution.py:101
  179.8 0.6 dynamic_slice.34
  181.1 2.3 conditional.3
  182.4 1.0 convolution_add_fusion
  185.6 0.9 copy-done.3
  186.5 2.0 convolution_convert_fusion.1
  188.6 75.0 %reduce-scatter.6.cloned.1.call-done = bf16[1,1024,512]{2,1,0:T(8,128)(2,1)} async-done(((bf16[1,1024,4096]{2,1,0:T(8,128)(2,1)}), bf16[1,1024,512]{2,1,0:T(8,128)(2,1)}) %reduce-scatter.6.cloned.1.call-update) | async-done | bytes 1048592 | tf_op jit(solution)/shard_map/reduce_scatter | solution.py:174
  263.5 16.0 %all_to_all.11 = bf16[4,256,512]{2,1,0:T(8,128)(2,1)S(1)} all-to-all(bf16[4,256,512]{2,1,0:T(8,128)(2,1)} %bitcast.120), channel_id=1, replica_groups=mesh['ep'=4,'tp'=8] {'ep'}, dimensions={0} | all-to-all | bytes 2097152 | tf_op jit(solution)/shard_map/all_to_all | solution.py:188
  279.5 0.7 fusion.42
  280.3 19.9 %reduce-scatter.8.cloned.1.call-done = bf16[256,512]{1,0:T(8,128)(2,1)} async-done(((bf16[256,4096]{1,0:T(8,128)(2,1)}), bf16[256,512]{1,0:T(8,128)(2,1)}) %reduce-scatter.8.cloned.1.call-update) | async-done | bytes 262160 | tf_op jit(solution)/shard_map/reduce_scatter | solution.py:235
  300.2 1.7 add_convert_fusion
  301.9 35.6 %reduce-scatter.4.cloned.1.call-done = bf16[256,512]{1,0:T(8,128)(2,1)} async-done(((bf16[256,4096]{1,0:T(8,128)(2,1)}), bf16[256,512]{1,0:T(8,128)(2,1)}) %reduce-scatter.4.cloned.1.call-update) | async-done | bytes 262160 | tf_op jit(solution)/shard_map/reduce_scatter | solution.py:232
  (75 shorter events, 5.7 us)
Async XLA Ops:
  7.2 142.2 %copy-start = (bf16[256,4096]{1,0:T(8,128)(2,1)S(1)}, bf16[256,4096]{1,0:T(8,128)(2,1)}, u32[]{:S(2)}) copy-start(bf16[256,4096]{1,0:T(8,128)(2,1)} %param.33) | copy-start | bytes 6291460
  7.2 107.0 %all-gather.7.cloned.1.call-start = ((), (), s32[]{:S(2)}) async-start(), calls=%async_computation.7 | async-start | bytes 9437184 | tf_op jit(solution)/shard_map/all_gather | solution.py:152
  12.8 20.2 %copy-start.5 = (bf16[256,256]{1,0:T(8,128)(2,1)S(1)}, bf16[256,256]{1,0:T(8,128)(2,1)}, u32[]{:S(2)}) copy-start(bf16[256,256]{1,0:T(8,128)(2,1)} %param.20) | copy-start | bytes 393220
  12.8 20.3 %copy-start.6 = (bf16[256,256]{1,0:T(8,128)(2,1)S(1)}, bf16[256,256]{1,0:T(8,128)(2,1)}, u32[]{:S(2)}) copy-start(bf16[256,256]{1,0:T(8,128)(2,1)} %param.19) | copy-start | bytes 393220
  32.2 1.5 copy-start.7
  32.2 112.6 %all-gather.9.cloned.1.call-start = ((), (), s32[]{:S(2)}) async-start(), calls=%async_computation.10 | async-start | bytes 2359296 | tf_op jit(solution)/shard_map/all_gather | solution.py:153
  33.0 138.8 %all-gather.5.cloned.1.call-start = ((), (), s32[]{:S(2)}) async-start(), calls=%async_computation.5 | async-start | bytes 1310720 | tf_op jit(solution)/shard_map/all_gather | solution.py:30
  34.5 229.0 %reduce-scatter.6.cloned.1.call-start = ((), (), s32[]{:S(2)}) async-start(), calls=%async_computation.8 | async-start | bytes 9437184 | tf_op jit(solution)/shard_map/reduce_scatter | solution.py:174
  114.2 5.8 %copy-start.2 = (bf16[1,1024,4096]{2,1,0:T(8,128)(2,1)S(1)}, bf16[1,1024,4096]{2,1,0:T(8,128)(2,1)}, u32[]{:S(2)}) copy-start(bf16[1,1024,4096]{2,1,0:T(8,128)(2,1)} %all-gather.7.cloned.1.call-done) | copy-start | bytes 25165828
  144.5 155.6 %reduce-scatter.8.cloned.1.call-start = ((), (), s32[]{:S(2)}) async-start(), calls=%async_computation.9 | async-start | bytes 2359296 | tf_op jit(solution)/shard_map/reduce_scatter | solution.py:235
  144.8 2.3 copy-start.1
  155.4 182.1 %reduce-scatter.4.cloned.1.call-start = ((), (), s32[]{:S(2)}) async-start(), calls=%async_computation.6 | async-start | bytes 2359296 | tf_op jit(solution)/shard_map/reduce_scatter | solution.py:232
  181.2 1.1 copy-start.4
  184.7 0.7 copy-start.8
  184.7 0.8 copy-start.9
  184.9 1.6 copy-start.3
  188.5 91.0 %copy-start.10 = (f32[256,2]{0,1:T(2,128)S(1)}, f32[256,2]{0,1:T(2,128)}, u32[]{:S(2)}) copy-start(f32[256,2]{0,1:T(2,128)} %param.27) | copy-start | bytes 6148
Sparse Core Ops, SparseCore 0:
  32.4 81.7 all-gather.6
  115.8 27.6 all-gather.8
  145.9 25.8 all-gather.4
  173.9 89.5 reduce-scatter.5
  265.6 34.5 reduce-scatter.7
  302.9 34.5 reduce-scatter.3
